TPU v7x, 32 devices: a whole 2x2x4 slice. The times are simulated.
32 devices in a mesh: ep: 16 (over z, y, core), tp: 2 (over x).
Axes of the slice: x: 2, y: 2, z: 4, core: 2. Of those that a mesh axis runs over, the one named last changes fastest.
Arguments:
- tokens: bfloat16 [128, 1024], P(('ep', 'tp')), may hold values from -6 to 6
- lengths: int32 [128], P(('ep', 'tp')), may hold values from 256 to 1024, as said below
- cache_latent: bfloat16 [128, 1024, 256], P(('ep', 'tp')), may hold values from -160 to 160
- cache_rope: bfloat16 [128, 32, 1024], P(('ep', 'tp')), may hold values from -6 to 6
- attn_gain: float32 [1024], replicated, may hold values from 0.1 to 1.9
- latent_gain: float32 [256], replicated, may hold values from 0.1 to 1.9
- post_gain: float32 [1024], replicated, may hold values from 0.1 to 1.9
- ffn_gain: float32 [1024], replicated, may hold values from 0.1 to 1.9
- out_gain: float32 [1024], replicated, may hold values from 0.1 to 1.9
- w_latent: bfloat16 [1024, 256], P(None, 'tp'), may hold values from -0.1875 to 0.1875
- w_rope_key: bfloat16 [1024, 32], replicated, may hold values from -0.1875 to 0.1875
- w_query: bfloat16 [1024, 768], P(None, 'tp'), may hold values from -0.1875 to 0.1875
- w_absorb_key: bfloat16 [8, 64, 256], P('tp'), may hold values from -0.75 to 0.75
- w_absorb_value: bfloat16 [8, 256, 64], P('tp'), may hold values from -0.375 to 0.375
- w_out: bfloat16 [512, 1024], P('tp'), may hold values from -0.25 to 0.25
- routes: int32 [128, 6], P(('ep', 'tp')), may hold values from 0 to 15, all different within a row; in each aligned block of 8 rows (0 to 7, 8 to 15, ...) at most 5 rows name the same one
- route_weights: float32 [128, 6], P(('ep', 'tp')), may hold values from 0.2 to 1
- w_exp_gate: bfloat16 [16, 1024, 256], P('ep'), may hold values from -0.1875 to 0.1875
- w_exp_up: bfloat16 [16, 1024, 256], P('ep'), may hold values from -0.1875 to 0.1875
- w_exp_down: bfloat16 [16, 256, 1024], P('ep'), may hold values from -0.375 to 0.375
- w_dense_gate: bfloat16 [4096, 1024], P('ep'), may hold values from -0.1875 to 0.1875
- w_dense_up: bfloat16 [4096, 1024], P('ep'), may hold values from -0.1875 to 0.1875
- w_dense_down: bfloat16 [4096, 1024], P('ep'), may hold values from -0.09375 to 0.09375
- dense_gate_vector: float32 [1024], replicated, may hold values from -0.1875 to 0.1875
Outputs:
- output: bfloat16 [128, 1024], P(('ep', 'tp'))
- new_latent: bfloat16 [128, 256], P(('ep', 'tp'))
- new_rope_key: bfloat16 [128, 32], P(('ep', 'tp'))
Inputs may be any that keep to these rules, and one draw needn't show every extreme that they name: `routes`: in each aligned block of 8 rows no expert is named by more than 5 rows; each row names 6 different experts. `lengths`: some sequence holds exactly 1024 cached positions.
All inputs are finite; a program needn't handle non-finite values.
Results may differ from a plain program's by a relative error of at most 0.015.
Values may be sent and summed in bfloat16 or wider, within the bound.
No kernel may reach another device: no remote copies, remote signals or barrier semaphores. Data moves between devices by JAX's collectives and lax.ppermute only.
A program may use at most 64 MiB of HBM per device.

v0:
```python
import jax
import jax.numpy as jnp
from jax import lax
from jax.sharding import PartitionSpec as P

epsilon = 1e-06
rope_base = 10000.0
negative = -1e30


def normalize(values, gain_vec):
    values = values.astype(jnp.float32)
    return (
        values * lax.rsqrt(jnp.mean(values * values, axis=-1, keepdims=True) + epsilon) * gain_vec
    )


def rotate(values, positions):
    half_width = values.shape[-1] // 2
    inverse = rope_base ** (-jnp.arange(half_width, dtype=jnp.float32) / half_width)
    angles = positions.astype(jnp.float32)[..., None] * inverse
    cosine = jnp.cos(angles)
    sine_part = jnp.sin(angles)
    first_half = values[..., :half_width]
    second = values[..., half_width:]
    return jnp.concatenate(
        [first_half * cosine - second * sine_part, first_half * sine_part + second * cosine],
        axis=-1,
    )


def attend(q_latent, q_rope, cache_lat, cache_rot, new_lat, new_rot, seq_lengths, scaling):
    scores = jnp.einsum("shc,slc->shl", q_latent, cache_lat, preferred_element_type=jnp.float32)
    scores = scores + jnp.einsum(
        "shr,srl->shl", q_rope, cache_rot, preferred_element_type=jnp.float32
    )
    scores = scores * scaling
    own_score = jnp.sum(
        q_latent.astype(jnp.float32) * new_lat.astype(jnp.float32)[:, None, :], axis=-1
    )
    own_score = (
        own_score
        + jnp.sum(q_rope.astype(jnp.float32) * new_rot.astype(jnp.float32)[:, None, :], axis=-1)
    ) * scaling
    visible = (
        jnp.arange(cache_lat.shape[1], dtype=jnp.int32)[None, None, :] < seq_lengths[:, None, None]
    )
    scores = jnp.where(visible, scores, negative)
    row_max = jnp.maximum(jnp.max(scores, axis=-1), own_score)
    weights = jnp.exp(scores - row_max[..., None])
    own_weight = jnp.exp(own_score - row_max)
    totals = jnp.sum(weights, axis=-1) + own_weight
    probabilities = (weights / totals[..., None]).astype(jnp.bfloat16)
    own_prob = (own_weight / totals).astype(jnp.bfloat16)
    mixed = jnp.einsum("shl,slc->shc", probabilities, cache_lat, preferred_element_type=jnp.float32)
    mixed = (
        mixed + own_prob.astype(jnp.float32)[..., None] * new_lat.astype(jnp.float32)[:, None, :]
    )
    return mixed.astype(jnp.bfloat16)


def expert_rows(rows_in, gate_w, up_w, down_w):
    model_width = rows_in.shape[-1]
    flattened = rows_in.reshape(-1, model_width)
    gate_pre = jnp.dot(flattened, gate_w, preferred_element_type=jnp.float32)
    up_proj = jnp.dot(flattened, up_w, preferred_element_type=jnp.float32)
    activity = (jax.nn.silu(gate_pre) * up_proj).astype(jnp.bfloat16)
    result = jnp.dot(activity, down_w, preferred_element_type=jnp.float32).astype(jnp.bfloat16)
    return result.reshape(rows_in.shape)


def rank_in_expert(flattened, experts):
    route_count = flattened.shape[0]
    onehot = (flattened[:, None] == jnp.arange(experts, dtype=jnp.int32)[None, :]).astype(
        jnp.float32
    )
    strictly = (jnp.arange(route_count)[:, None] > jnp.arange(route_count)[None, :]).astype(
        jnp.float32
    )
    earlier = jnp.dot(strictly, onehot, precision=lax.Precision.HIGHEST)
    return jnp.sum(earlier * onehot, axis=1).astype(jnp.int32)


def shards(
    tokens,
    lengths,
    cache_latent,
    cache_rope,
    attn_gain,
    latent_gain,
    post_gain,
    ffn_gain,
    out_gain,
    w_latent,
    w_rope_key,
    w_query,
    w_absorb_key,
    w_absorb_value,
    w_out,
    routes,
    route_weights,
    w_exp_gate,
    w_exp_up,
    w_exp_down,
    w_dense_gate,
    w_dense_up,
    w_dense_down,
    dense_gate_vector,
):
    own_rows = tokens.shape[0]
    model_width = tokens.shape[1]
    tp_count = lax.axis_size("tp")
    ep_count = lax.axis_size("ep")
    rope_width = w_rope_key.shape[1]
    nope_width = w_absorb_key.shape[1]
    head_span = nope_width + rope_width
    scaling = head_span ** (-0.5)
    top_count = routes.shape[1]
    group_size = own_rows * tp_count
    capacity = min(
        group_size, max(2, (3 * group_size * top_count + 2 * ep_count - 1) // (2 * ep_count))
    )
    hidden = normalize(tokens, attn_gain).astype(jnp.bfloat16)
    new_rope_key = rotate(
        jnp.dot(hidden, w_rope_key, preferred_element_type=jnp.float32), lengths
    ).astype(jnp.bfloat16)
    local_heads = w_absorb_key.shape[0]
    group_hidden = lax.all_gather(hidden, "tp", axis=0, tiled=True)
    latent_part = jnp.dot(group_hidden, w_latent, preferred_element_type=jnp.float32)
    latent_full = lax.all_to_all(latent_part, "tp", split_axis=0, concat_axis=1, tiled=True)
    new_latent = normalize(latent_full, latent_gain).astype(jnp.bfloat16)
    queries = jnp.dot(group_hidden, w_query, preferred_element_type=jnp.float32).astype(
        jnp.bfloat16
    )
    queries = queries.reshape(group_size, local_heads, head_span)
    query_latent = jnp.einsum(
        "shn,hnc->shc", queries[..., :nope_width], w_absorb_key, preferred_element_type=jnp.float32
    ).astype(jnp.bfloat16)
    query_latent, query_rope = (
        lax.all_to_all(query_latent, "tp", split_axis=0, concat_axis=1, tiled=True),
        lax.all_to_all(queries[..., nope_width:], "tp", split_axis=0, concat_axis=1, tiled=True),
    )
    query_rope = rotate(query_rope.astype(jnp.float32), lengths[:, None]).astype(jnp.bfloat16)
    attended = attend(
        query_latent,
        query_rope,
        cache_latent,
        cache_rope,
        new_latent,
        new_rope_key,
        lengths,
        scaling,
    )
    attended = lax.all_to_all(attended, "tp", split_axis=1, concat_axis=0, tiled=True)
    head_out = (
        jnp.einsum("shc,hcv->shv", attended, w_absorb_value, preferred_element_type=jnp.float32)
        .astype(jnp.bfloat16)
        .reshape(group_size, -1)
    )
    mixed = lax.psum_scatter(
        jnp.dot(head_out, w_out, preferred_element_type=jnp.float32).astype(jnp.bfloat16),
        "tp",
        scatter_dimension=0,
        tiled=True,
    ).astype(jnp.float32)
    residual = (tokens.astype(jnp.float32) + normalize(mixed, post_gain)).astype(jnp.bfloat16)
    ffn_in = normalize(residual, ffn_gain).astype(jnp.bfloat16)
    gate_w = w_exp_gate[0]
    up_w = w_exp_up[0]
    down_w = w_exp_down[0]
    flattened = routes.reshape(-1)
    order_rank = rank_in_expert(flattened, ep_count)
    slot_index = (flattened * capacity + order_rank).reshape(own_rows, top_count)
    dispatch = jnp.any(
        slot_index[None, :, :] == jnp.arange(ep_count * capacity, dtype=jnp.int32)[:, None, None],
        axis=-1,
    ).astype(jnp.bfloat16)
    outgoing = jnp.dot(dispatch, ffn_in, preferred_element_type=jnp.float32).astype(jnp.bfloat16)
    outgoing = outgoing.reshape(ep_count, capacity, model_width)
    result = expert_rows(
        lax.all_to_all(outgoing, "ep", split_axis=0, concat_axis=0, tiled=True),
        gate_w,
        up_w,
        down_w,
    )
    returned = lax.all_to_all(result, "ep", split_axis=0, concat_axis=0, tiled=True)
    picked = returned.reshape(ep_count * capacity, model_width)[slot_index].astype(jnp.float32)
    routed = jnp.sum(route_weights[..., None] * picked, axis=1)
    piece_rows = lax.all_gather(ffn_in, "ep", axis=0, tiled=True)
    dims = (((1,), (1,)), ((), ()))
    gate_pre = lax.dot_general(piece_rows, w_dense_gate, dims, preferred_element_type=jnp.float32)
    up_proj = lax.dot_general(piece_rows, w_dense_up, dims, preferred_element_type=jnp.float32)
    dense_act = (jax.nn.silu(gate_pre) * up_proj).astype(jnp.bfloat16)
    dense_out = lax.psum_scatter(
        jnp.dot(dense_act, w_dense_down, preferred_element_type=jnp.float32),
        "ep",
        scatter_dimension=0,
        tiled=True,
    )
    dense_gate = jax.nn.sigmoid(jnp.sum(ffn_in.astype(jnp.float32) * dense_gate_vector, axis=-1))
    combined = routed + dense_gate[:, None] * dense_out
    output = (residual.astype(jnp.float32) + normalize(combined, out_gain)).astype(jnp.bfloat16)
    return (output, new_latent, new_rope_key)


def solution(mesh):
    placed = (
        P(("ep", "tp"), None),
        P(("ep", "tp")),
        P(("ep", "tp"), None, None),
        P(("ep", "tp"), None, None),
        P(),
        P(),
        P(),
        P(),
        P(),
        P(None, "tp"),
        P(),
        P(None, "tp"),
        P("tp", None, None),
        P("tp", None, None),
        P("tp", None),
        P(("ep", "tp"), None),
        P(("ep", "tp"), None),
        P("ep", None, None),
        P("ep", None, None),
        P("ep", None, None),
        P("ep", None),
        P("ep", None),
        P("ep", None),
        P(),
    )
    return jax.shard_map(
        shards,
        mesh=mesh,
        in_specs=placed,
        out_specs=(P(("ep", "tp"), None), P(("ep", "tp"), None), P(("ep", "tp"), None)),
        check_vma=False,
    )
```

profile of v0, /device:TPU:0, one launch (start us, length us, event | category | flops | bytes accessed | tf_op | source)
XLA Modules:
  0.0 204.9 jit_solution(364668685929764041)
XLA Ops:
  7.2 1.0 fusion.31
  8.2 0.8 fusion.54
  9.0 5.3 %all-gather = bf16[2,4,1024]{2,1,0:T(4,128)(2,1)S(1)} all-gather(bf16[1,4,1024]{2,1,0:T(4,128)(2,1)S(1)} %fusion.54), channel_id=1, replica_groups=mesh['ep'=16,'tp'=2] {'tp'}, dimensions={0}, use_global_device_ids=true | all-gather | bytes 24576 | tf_op jit(solution)/shard_map/all_gather | solution.py:128
  14.2 1.3 convolution_convert_fusion.5
  15.8 0.7 reshape.295
  16.4 3.3 %all-to-all-start.1 = ((bf16[2,2,256]{2,1,0:T(2,128)(2,1)}), bf16[2,2,256]{2,1,0:T(2,128)(2,1)S(1)}, u32[]{:S(2)}, u32[]{:S(2)}) async-start(bf16[2,2,256]{2,1,0:T(2,128)(2,1)} %reshape.295), calls=%async_computation.1 | async-start | bytes 4096 | tf_op jit(solution)/shard_map/all_to_all | solution.py:141
  19.8 0.7 convert_element_type.152
  20.4 0.7 iota_compare_fusion
  21.1 1.1 fusion.52
  22.2 1.7 fusion.62
  23.9 0.8 eq.28
  24.9 0.7 compare_select_fusion
  25.6 1.0 fusion.6
  26.7 0.6 fusion.57
  27.4 0.6 copy.49
  28.1 3.3 %all-to-all-start.2 = ((f32[2,4,128]{2,1,0:T(4,128)}), f32[2,4,128]{2,1,0:T(4,128)S(1)}, u32[]{:S(2)}, u32[]{:S(2)}) async-start(f32[2,4,128]{2,1,0:T(4,128)} %bitcast.9), calls=%async_computation.2 | async-start | bytes 8192 | tf_op jit(solution)/shard_map/all_to_all | solution.py:130
  31.7 3.5 %all-to-all-done.2 = f32[2,4,128]{2,1,0:T(4,128)S(1)} async-done(((f32[2,4,128]{2,1,0:T(4,128)}), f32[2,4,128]{2,1,0:T(4,128)S(1)}, u32[]{:S(2)}, u32[]{:S(2)}) %all-to-all-start.2) | async-done | bytes 4128 | tf_op jit(solution)/shard_map/all_to_all | solution.py:130
  35.2 3.2 %all-to-all-start = ((bf16[8,4,256]{2,1,0:T(4,128)(2,1)}), bf16[8,4,256]{2,1,0:T(4,128)(2,1)S(1)}, u32[]{:S(2)}, u32[]{:S(2)}) async-start(bf16[8,4,256]{2,1,0:T(4,128)(2,1)} %copy.49), calls=%async_computation | async-start | bytes 32768 | tf_op jit(solution)/shard_map/all_to_all | solution.py:140
  38.5 1.3 fusion.58
  39.9 2.4 %all-to-all-done = bf16[8,4,256]{2,1,0:T(4,128)(2,1)S(1)} async-done(((bf16[8,4,256]{2,1,0:T(4,128)(2,1)}), bf16[8,4,256]{2,1,0:T(4,128)(2,1)S(1)}, u32[]{:S(2)}, u32[]{:S(2)}) %all-to-all-start) | async-done | bytes 16416 | tf_op jit(solution)/shard_map/all_to_all | solution.py:140
  42.6 0.6 fusion.61
  43.3 0.3 fusion.60
  43.6 0.2 fusion.14
  43.8 0.4 fusion.5
  44.2 0.6 copy.55
  44.8 3.2 %all-to-all-start.3 = ((bf16[4,8,256]{2,0,1:T(4,128)(2,1)}), bf16[4,8,256]{2,0,1:T(4,128)(2,1)S(1)}, u32[]{:S(2)}, u32[]{:S(2)}) async-start(bf16[4,8,256]{2,0,1:T(4,128)(2,1)} %copy.55), calls=%async_computation.3 | async-start | bytes 32768 | tf_op jit(solution)/shard_map/all_to_all | solution.py:154
  48.3 0.6 dynamic-slice
  49.5 2.4 %all-to-all-done.3 = bf16[4,8,256]{2,0,1:T(4,128)(2,1)S(1)} async-done(((bf16[4,8,256]{2,0,1:T(4,128)(2,1)}), bf16[4,8,256]{2,0,1:T(4,128)(2,1)S(1)}, u32[]{:S(2)}, u32[]{:S(2)}) %all-to-all-start.3) | async-done | bytes 16416 | tf_op jit(solution)/shard_map/all_to_all | solution.py:154
  52.2 0.2 convolution_convert_fusion.3
  52.4 6.7 %all-reduce = bf16[8,1024]{1,0:T(8,128)(2,1)S(1)} all-reduce(bf16[8,1024]{1,0:T(8,128)(2,1)S(1)} %convolution_convert_fusion.3), channel_id=2, replica_groups=mesh['ep'=16,'tp'=2] {'tp'}, use_global_device_ids=true, to_apply=%region_6.7.clone | all-reduce | flops 8192 | bytes 32768
  59.3 0.2 fusion.35
  59.5 0.7 multiply_reduce_fusion.3
  60.2 0.2 convolution_convert_fusion.1
  60.5 0.8 reshape.272
  61.2 6.4 %all-to-all-start.4 = ((bf16[16,5,1024]{2,1,0:T(8,128)(2,1)}), bf16[16,5,1024]{2,1,0:T(8,128)(2,1)S(1)}, u32[]{:S(2)}, u32[]{:S(2)}) async-start(bf16[16,5,1024]{2,1,0:T(8,128)(2,1)} %reshape.272), calls=%async_computation.4 | async-start | bytes 524288 | tf_op jit(solution)/shard_map/all_to_all | solution.py:181
  67.6 1.3 dynamic-slice.2
  69.6 22.1 %all-gather.1 = bf16[16,4,1024]{2,1,0:T(4,128)(2,1)S(1)} all-gather(bf16[1,4,1024]{2,1,0:T(4,128)(2,1)S(1)} %bitcast.76), channel_id=1, replica_groups=mesh['ep'=16,'tp'=2] {'ep'}, dimensions={0}, use_global_device_ids=true | all-gather | bytes 139264 | tf_op jit(solution)/shard_map/all_gather | solution.py:189
  91.7 0.9 fusion.63
  92.7 1.3 fusion.12
  93.9 1.7 convolution_convert_fusion
  95.7 0.8 reshape.274
  96.4 3.5 %all-to-all-start.5 = ((bf16[16,5,1024]{2,1,0:T(8,128)(2,1)}), bf16[16,5,1024]{2,1,0:T(8,128)(2,1)S(1)}, u32[]{:S(2)}, u32[]{:S(2)}) async-start(bf16[16,5,1024]{2,1,0:T(8,128)(2,1)} %reshape.274), calls=%async_computation.5 | async-start | bytes 524288 | tf_op jit(solution)/shard_map/all_to_all | solution.py:186
  100.0 2.3 %fusion.4 = f32[64,1024]{1,0:T(8,128)} fusion(bf16[256,1024]{1,0:T(8,128)(2,1)S(1)} %copy-done.1, bf16[64,1024]{1,0:T(8,128)(2,1)S(1)} %reshape.292, bf16[256,1024]{1,0:T(8,128)(2,1)} %param.45, f32[64,256]{1,0:T(8,128)S(1)} %copy-done.5), kind=kOutput, calls=%fused_computation.10 | convolution fusion | flops 67207168 | bytes 1507328 | tf_op jit(solution)/shard_map/dot_general | solution.py:195
  102.4 7.5 %all-to-all-done.5 = bf16[16,5,1024]{2,1,0:T(8,128)(2,1)S(1)} async-done(((bf16[16,5,1024]{2,1,0:T(8,128)(2,1)}), bf16[16,5,1024]{2,1,0:T(8,128)(2,1)S(1)}, u32[]{:S(2)}, u32[]{:S(2)}) %all-to-all-start.5) | async-done | bytes 163872 | tf_op jit(solution)/shard_map/all_to_all | solution.py:186
  110.0 0.6 gather_fusion
  110.8 84.8 %all-reduce.4.cloned.1.call-done = f32[64,1024]{1,0:T(8,128)} async-done(((f32[64,1024]{1,0:T(8,128)}), f32[64,1024]{1,0:T(8,128)}) %all-reduce.4.cloned.1.call-update) | async-done | bytes 262160
  195.6 0.9 multiply_reduce_fusion.2
  196.6 1.4 fusion.38
  (75 shorter events, 2.5 us)
Async XLA Ops:
  7.2 35.4 %copy-start = (bf16[4,1024,256]{2,1,0:T(8,128)(2,1)S(1)}, bf16[4,1024,256]{2,1,0:T(8,128)(2,1)}, u32[]{:S(2)}) copy-start(bf16[4,1024,256]{2,1,0:T(8,128)(2,1)} %param.26) | copy-start | bytes 6291460
  7.2 36.0 %copy-start.4 = (bf16[4,32,1024]{2,1,0:T(8,128)(2,1)S(1)}, bf16[4,32,1024]{2,1,0:T(8,128)(2,1)}, u32[]{:S(2)}) copy-start(bf16[4,32,1024]{2,1,0:T(8,128)(2,1)} %param.27) | copy-start | bytes 786436
  16.4 11.7 %all-to-all-start.1 = ((bf16[2,2,256]{2,1,0:T(2,128)(2,1)}), bf16[2,2,256]{2,1,0:T(2,128)(2,1)S(1)}, u32[]{:S(2)}, u32[]{:S(2)}) async-start(bf16[2,2,256]{2,1,0:T(2,128)(2,1)} %reshape.295), calls=%async_computation.1 | async-start | bytes 4096 | tf_op jit(solution)/shard_map/all_to_all | solution.py:141
  28.1 7.1 %all-to-all-start.2 = ((f32[2,4,128]{2,1,0:T(4,128)}), f32[2,4,128]{2,1,0:T(4,128)S(1)}, u32[]{:S(2)}, u32[]{:S(2)}) async-start(f32[2,4,128]{2,1,0:T(4,128)} %bitcast.9), calls=%async_computation.2 | async-start | bytes 8192 | tf_op jit(solution)/shard_map/all_to_all | solution.py:130
  35.2 7.1 %all-to-all-start = ((bf16[8,4,256]{2,1,0:T(4,128)(2,1)}), bf16[8,4,256]{2,1,0:T(4,128)(2,1)S(1)}, u32[]{:S(2)}, u32[]{:S(2)}) async-start(bf16[8,4,256]{2,1,0:T(4,128)(2,1)} %copy.49), calls=%async_computation | async-start | bytes 32768 | tf_op jit(solution)/shard_map/all_to_all | solution.py:140
  42.6 5.7 %copy-start.14 = (u32[32]{0:T(128)S(1)}, u32[32]{0:T(128)}, u32[]{:S(2)}) copy-start(u32[32]{0:T(128)} %constant.51) | copy-start | bytes 388
  43.2 8.7 %copy-start.6 = (bf16[4,256,64]{1,2,0:T(8,128)(2,1)S(1)}, bf16[4,256,64]{1,2,0:T(8,128)(2,1)}, u32[]{:S(2)}) copy-start(bf16[4,256,64]{1,2,0:T(8,128)(2,1)} %param.37) | copy-start | bytes 393220
  43.2 9.0 %copy-start.2 = (bf16[256,1024]{1,0:T(8,128)(2,1)S(1)}, bf16[256,1024]{1,0:T(8,128)(2,1)}, u32[]{:S(2)}) copy-start(bf16[256,1024]{1,0:T(8,128)(2,1)} %param.38) | copy-start | bytes 1572868
  43.2 16.0 %copy-start.7 = (bf16[4,1024]{1,0:T(4,128)(2,1)S(1)}, bf16[4,1024]{1,0:T(4,128)(2,1)}, u32[]{:S(2)}) copy-start(bf16[4,1024]{1,0:T(4,128)(2,1)} %param.24) | copy-start | bytes 24580
  43.2 16.0 %copy-start.10 = (f32[1024]{0:T(1024)S(1)}, f32[1024]{0:T(1024)}, u32[]{:S(2)}) copy-start(f32[1024]{0:T(1024)} %param.30) | copy-start | bytes 12292
  43.3 16.2 %copy-start.8 = (f32[1024]{0:T(1024)S(1)}, f32[1024]{0:T(1024)}, u32[]{:S(2)}) copy-start(f32[1024]{0:T(1024)} %param.47) | copy-start | bytes 12292
  43.3 16.2 %copy-start.9 = (f32[1024]{0:T(1024)S(1)}, f32[1024]{0:T(1024)}, u32[]{:S(2)}) copy-start(f32[1024]{0:T(1024)} %param.31) | copy-start | bytes 12292
  43.8 47.9 %copy-start.3 = (bf16[256,1024]{1,0:T(8,128)(2,1)S(1)}, bf16[256,1024]{1,0:T(8,128)(2,1)}, u32[]{:S(2)}) copy-start(bf16[256,1024]{1,0:T(8,128)(2,1)} %param.44) | copy-start | bytes 1572868
  44.8 7.1 %all-to-all-start.3 = ((bf16[4,8,256]{2,0,1:T(4,128)(2,1)}), bf16[4,8,256]{2,0,1:T(4,128)(2,1)S(1)}, u32[]{:S(2)}, u32[]{:S(2)}) async-start(bf16[4,8,256]{2,0,1:T(4,128)(2,1)} %copy.55), calls=%async_computation.3 | async-start | bytes 32768 | tf_op jit(solution)/shard_map/all_to_all | solution.py:154
  61.2 31.4 %all-to-all-start.4 = ((bf16[16,5,1024]{2,1,0:T(8,128)(2,1)}), bf16[16,5,1024]{2,1,0:T(8,128)(2,1)S(1)}, u32[]{:S(2)}, u32[]{:S(2)}) async-start(bf16[16,5,1024]{2,1,0:T(8,128)(2,1)} %reshape.272), calls=%async_computation.4 | async-start | bytes 524288 | tf_op jit(solution)/shard_map/all_to_all | solution.py:181
  91.7 8.4 %copy-start.1 = (bf16[256,1024]{1,0:T(8,128)(2,1)S(1)}, bf16[256,1024]{1,0:T(8,128)(2,1)}, u32[]{:S(2)}) copy-start(bf16[256,1024]{1,0:T(8,128)(2,1)} %param.46) | copy-start | bytes 1572868
  92.6 7.5 %copy-start.5 = (f32[64,256]{1,0:T(8,128)S(1)}, f32[64,256]{1,0:T(8,128)}, u32[]{:S(2)}) copy-start(f32[64,256]{1,0:T(8,128)} %fusion.63) | copy-start | bytes 196612
  93.9 8.5 %copy-start.13 = (f32[4]{0:T(128)S(1)}, f32[4]{0:T(128)}, u32[]{:S(2)}) copy-start(f32[4]{0:T(128)} %get-tuple-element.3) | copy-start | bytes 52
  95.7 15.0 %copy-start.12 = (f32[4,6]{1,0:T(4,128)S(1)}, f32[4,6]{1,0:T(4,128)}, u32[]{:S(2)}) copy-start(f32[4,6]{1,0:T(4,128)} %param.40) | copy-start | bytes 292
  95.7 100.9 %copy-start.11 = (f32[1024]{0:T(1024)S(1)}, f32[1024]{0:T(1024)}, u32[]{:S(2)}) copy-start(f32[1024]{0:T(1024)} %param.32) | copy-start | bytes 12292
  96.4 13.5 %all-to-all-start.5 = ((bf16[16,5,1024]{2,1,0:T(8,128)(2,1)}), bf16[16,5,1024]{2,1,0:T(8,128)(2,1)S(1)}, u32[]{:S(2)}, u32[]{:S(2)}) async-start(bf16[16,5,1024]{2,1,0:T(8,128)(2,1)} %reshape.274), calls=%async_computation.5 | async-start | bytes 524288 | tf_op jit(solution)/shard_map/all_to_all | solution.py:186
  100.0 95.7 %all-reduce.4.cloned.1.call-start = ((), (), s32[]{:S(2)}) async-start(), calls=%async_computation.6 | async-start | bytes 524288
Sparse Core Ops, SparseCore 0:
  104.2 91.4 all-reduce.3
where the time goes:
time: 206 us; the launch traced here: 205 us
  waiting for transfers between devices  101 us (49%)
  blocking collectives  34.1 us (17%)
  starting transfers between devices  23 us (11%)
  between operations  15.6 us (8%)
  matrix products  13.3 us (6%)
  other arithmetic  10.3 us (5%)
  local copies, waits for them, and re-layouts  7.86 us (4%)
    unnamed x2, waiting for transfers between devices  84.8 us
    all_gather x1, blocking collectives, shards(): piece_rows = lax.all_gather(ffn_in, 'ep', axis=0, tiled=True)  22.1 us
    all_to_all x1, waiting for transfers between devices, shards(): lax.all_to_all(result, 'ep', split_axis=0, concat_axis=0, tiled=True)  7.54 us
    unnamed x1, blocking collectives  6.72 us
    all_to_all x1, starting transfers between devices, shards(): lax.all_to_all(outgoing, 'ep', split_axis=0, concat_axis=0, tiled=True)  6.39 us
    all_gather x1, blocking collectives, shards(): group_hidden = lax.all_gather(hidden, 'tp', axis=0, tiled=True)  5.27 us
  transfers between devices with their start and end apart: 7, of which 5 were waited for; matrix products, arithmetic and copies ran while one was open for 8% of the time, Pallas kernels for 0%

commit v1 on v0

--- a/solution.py
+++ b/solution.py
@@ -6,6 +6,17 @@
 epsilon = 1e-06
 rope_base = 10000.0
 negative = -1e30
+
+
+def split_up(x, dim, size):
+    before, after = (x.shape[:dim], x.shape[dim + 1 :])
+    return jnp.moveaxis(x.reshape(*before, size, -1, *after), dim, 0)
+
+
+def joined_along(blocks, dim):
+    lengths = list(blocks.shape[1:])
+    lengths[dim] *= blocks.shape[0]
+    return jnp.moveaxis(blocks, 0, dim).reshape(lengths)
 
 
 def normalize(values, gain_vec):
@@ -183,7 +194,14 @@
         up_w,
         down_w,
     )
-    returned = lax.all_to_all(result, "ep", split_axis=0, concat_axis=0, tiled=True)
+    peers, place = (lax.axis_size("ep"), lax.axis_index("ep"))
+    pieces = split_up(result, 0, peers)
+    outs = [pieces[place]]
+    for step in range(1, peers):
+        sent = pieces[place ^ step]
+        outs.append(lax.ppermute(sent, "ep", [(i, i ^ step) for i in range(peers)]))
+    pieces = jnp.stack(outs)[place ^ jnp.arange(peers)]
+    returned = joined_along(pieces, 0)
     picked = returned.reshape(ep_count * capacity, model_width)[slot_index].astype(jnp.float32)
     routed = jnp.sum(route_weights[..., None] * picked, axis=1)
     piece_rows = lax.all_gather(ffn_in, "ep", axis=0, tiled=True)

time: 206 us -> 196 us (0.951)
  waiting for transfers between devices: 101 us -> 69.4 us
  starting transfers between devices: 23 us -> 39.9 us
  blocking collectives: 34.1 us -> 36.3 us
    unnamed x2, waiting for transfers between devices: 84.8 us -> 60.1 us
    ppermute x0 -> x15, starting transfers between devices: none -> 20.4 us  [shards(): outs.append(lax.ppermute(sent, 'ep', [(i, i ^ step) for i in range(peers)]))]
    all_to_all x1 -> x0, waiting for transfers between devices: 7.54 us -> none  [shards(): lax.all_to_all(result, 'ep', split_axis=0, concat_axis=0, tiled=True)]
    all_to_all x1 -> x0, starting transfers between devices: 3.53 us -> none  [shards(): lax.all_to_all(result, 'ep', split_axis=0, concat_axis=0, tiled=True)]
    ppermute x0 -> x15, waiting for transfers between devices: none -> 2.42 us  [shards(): outs.append(lax.ppermute(sent, 'ep', [(i, i ^ step) for i in range(peers)]))]
  transfers between devices with their start and end apart: 7 -> 21, of which waited for: 5 -> 6; matrix products, arithmetic and copies ran while one was open for 8% -> 11% of each run, Pallas kernels for 0% -> 0%
where the time goes in v1:
time: 196 us; the launch traced here: 195 us
  waiting for transfers between devices  69.4 us (35%)
  starting transfers between devices  39.9 us (20%)
  blocking collectives  36.3 us (19%)
  between operations  15.9 us (8%)
  matrix products  15.2 us (8%)
  other arithmetic  10.3 us (5%)
  local copies, waits for them, and re-layouts  8.11 us (4%)
    unnamed x2, waiting for transfers between devices  60.1 us
    all_gather x1, blocking collectives, shards(): piece_rows = lax.all_gather(ffn_in, 'ep', axis=0, tiled=True)  23.6 us
    ppermute x15, starting transfers between devices, shards(): outs.append(lax.ppermute(sent, 'ep', [(i, i ^ step) for i in range(peers)]))  20.4 us
    unnamed x1, blocking collectives  7.5 us
    all_to_all x1, starting transfers between devices, shards(): lax.all_to_all(outgoing, 'ep', split_axis=0, concat_axis=0, tiled=True)  6.39 us
    all_gather x1, blocking collectives, shards(): group_hidden = lax.all_gather(hidden, 'tp', axis=0, tiled=True)  5.27 us
  transfers between devices with their start and end apart: 21, of which 6 were waited for; matrix products, arithmetic and copies ran while one was open for 11% of the time, Pallas kernels for 0%

profile of v1, /device:TPU:0, one launch (start us, length us, event | category | flops | bytes accessed | tf_op | source)
XLA Modules:
  0.0 195.2 jit_solution(4490124801480925766)
XLA Ops:
  7.2 1.0 fusion.31
  8.2 0.8 fusion.55
  9.0 5.3 %all-gather = bf16[2,4,1024]{2,1,0:T(4,128)(2,1)S(1)} all-gather(bf16[1,4,1024]{2,1,0:T(4,128)(2,1)S(1)} %fusion.55), channel_id=1, replica_groups=mesh['ep'=16,'tp'=2] {'tp'}, dimensions={0}, use_global_device_ids=true | all-gather | bytes 24576 | tf_op jit(solution)/shard_map/all_gather | solution.py:139
  14.2 1.3 convolution_convert_fusion.5
  15.8 0.7 reshape.314
  16.4 3.3 %all-to-all-start.1 = ((bf16[2,2,256]{2,1,0:T(2,128)(2,1)}), bf16[2,2,256]{2,1,0:T(2,128)(2,1)S(1)}, u32[]{:S(2)}, u32[]{:S(2)}) async-start(bf16[2,2,256]{2,1,0:T(2,128)(2,1)} %reshape.314), calls=%async_computation.1 | async-start | bytes 4096 | tf_op jit(solution)/shard_map/all_to_all | solution.py:152
  19.8 0.7 convert_element_type.152
  20.4 0.7 iota_compare_fusion
  21.1 1.1 fusion.53
  22.2 1.7 fusion.63
  23.9 0.8 eq.28
  24.9 0.7 compare_select_fusion
  25.8 1.0 fusion.6
  27.0 0.6 fusion.58
  27.6 0.6 copy.49
  28.3 3.3 %all-to-all-start.2 = ((f32[2,4,128]{2,1,0:T(4,128)}), f32[2,4,128]{2,1,0:T(4,128)S(1)}, u32[]{:S(2)}, u32[]{:S(2)}) async-start(f32[2,4,128]{2,1,0:T(4,128)} %bitcast.9), calls=%async_computation.2 | async-start | bytes 8192 | tf_op jit(solution)/shard_map/all_to_all | solution.py:141
  31.9 3.5 %all-to-all-done.2 = f32[2,4,128]{2,1,0:T(4,128)S(1)} async-done(((f32[2,4,128]{2,1,0:T(4,128)}), f32[2,4,128]{2,1,0:T(4,128)S(1)}, u32[]{:S(2)}, u32[]{:S(2)}) %all-to-all-start.2) | async-done | bytes 4128 | tf_op jit(solution)/shard_map/all_to_all | solution.py:141
  35.4 3.2 %all-to-all-start = ((bf16[8,4,256]{2,1,0:T(4,128)(2,1)}), bf16[8,4,256]{2,1,0:T(4,128)(2,1)S(1)}, u32[]{:S(2)}, u32[]{:S(2)}) async-start(bf16[8,4,256]{2,1,0:T(4,128)(2,1)} %copy.49), calls=%async_computation | async-start | bytes 32768 | tf_op jit(solution)/shard_map/all_to_all | solution.py:151
  38.7 1.3 fusion.59
  40.1 2.4 %all-to-all-done = bf16[8,4,256]{2,1,0:T(4,128)(2,1)S(1)} async-done(((bf16[8,4,256]{2,1,0:T(4,128)(2,1)}), bf16[8,4,256]{2,1,0:T(4,128)(2,1)S(1)}, u32[]{:S(2)}, u32[]{:S(2)}) %all-to-all-start) | async-done | bytes 16416 | tf_op jit(solution)/shard_map/all_to_all | solution.py:151
  42.8 0.6 fusion.62
  44.5 0.6 copy.55
  45.1 3.2 %all-to-all-start.3 = ((bf16[4,8,256]{2,0,1:T(4,128)(2,1)}), bf16[4,8,256]{2,0,1:T(4,128)(2,1)S(1)}, u32[]{:S(2)}, u32[]{:S(2)}) async-start(bf16[4,8,256]{2,0,1:T(4,128)(2,1)} %copy.55), calls=%async_computation.3 | async-start | bytes 32768 | tf_op jit(solution)/shard_map/all_to_all | solution.py:165
  49.0 0.7 dynamic-slice.2
  51.1 1.1 all-to-all-done.3
  52.4 1.2 convolution_convert_fusion.3
  53.7 7.5 %all-reduce = bf16[8,1024]{1,0:T(8,128)(2,1)S(1)} all-reduce(bf16[8,1024]{1,0:T(8,128)(2,1)S(1)} %convolution_convert_fusion.3), channel_id=2, replica_groups=mesh['ep'=16,'tp'=2] {'tp'}, use_global_device_ids=true, to_apply=%region_6.7.clone | all-reduce | flops 8192 | bytes 32768
  61.5 0.7 multiply_reduce_fusion.3
  62.5 0.8 reshape.282
  63.3 6.4 %all-to-all-start.4 = ((bf16[16,5,1024]{2,1,0:T(8,128)(2,1)}), bf16[16,5,1024]{2,1,0:T(8,128)(2,1)S(1)}, u32[]{:S(2)}, u32[]{:S(2)}) async-start(bf16[16,5,1024]{2,1,0:T(8,128)(2,1)} %reshape.282), calls=%async_computation.4 | async-start | bytes 524288 | tf_op jit(solution)/shard_map/all_to_all | solution.py:192
  69.7 23.6 %all-gather.1 = bf16[16,4,1024]{2,1,0:T(4,128)(2,1)} all-gather(bf16[1,4,1024]{2,1,0:T(4,128)(2,1)S(1)} %bitcast.140), channel_id=1, replica_groups=mesh['ep'=16,'tp'=2] {'ep'}, dimensions={0}, use_global_device_ids=true | all-gather | bytes 139264 | tf_op jit(solution)/shard_map/all_gather | solution.py:207
  93.3 0.9 reshape.311
  94.2 2.0 fusion.64
  96.2 2.1 %fusion.4 = f32[64,1024]{1,0:T(8,128)} fusion(bf16[256,1024]{1,0:T(8,128)(2,1)S(1)} %copy-done.1, bf16[64,1024]{1,0:T(8,128)(2,1)S(1)} %reshape.311, bf16[256,1024]{1,0:T(8,128)(2,1)S(1)} %copy-done.2, f32[64,256]{1,0:T(8,128)} %fusion.64), kind=kOutput, calls=%fused_computation.11 | convolution fusion | flops 67207168 | bytes 1507328 | tf_op jit(solution)/shard_map/dot_general | solution.py:213
  98.4 1.3 fusion.12
  99.7 1.7 convolution_convert_fusion
  102.5 1.1 collective-permute-start.2
  103.6 2.0 %collective-permute-start.4 = (bf16[1,5,1024]{2,1,0:T(8,128)(2,1)S(1)}, bf16[1,5,1024]{2,1,0:T(8,128)(2,1)S(1)}, u32[]{:S(2)}, u32[]{:S(2)}) collective-permute-start(bf16[1,5,1024]{2,1,0:T(8,128)(2,1)S(1)} %get-tuple-element.23), channel_id=1, source_target_pairs={{0,10},{2,8},{4,14},{6,12},{8,2},{10,0},{12,6},{14,4},{16,26},{18,... | collective-permute-start | bytes 30728 | tf_op jit(solution)/shard_map/ppermute | solution.py:202
  105.9 2.1 %collective-permute-start.6 = (bf16[1,5,1024]{2,1,0:T(8,128)(2,1)S(1)}, bf16[1,5,1024]{2,1,0:T(8,128)(2,1)S(1)}, u32[]{:S(2)}, u32[]{:S(2)}) collective-permute-start(bf16[1,5,1024]{2,1,0:T(8,128)(2,1)S(1)} %get-tuple-element.21), channel_id=1, source_target_pairs={{0,14},{2,12},{4,10},{6,8},{8,6},{10,4},{12,2},{14,0},{16,30},{18,... | collective-permute-start | bytes 30728 | tf_op jit(solution)/shard_map/ppermute | solution.py:202
  108.0 2.9 %collective-permute-start.8 = (bf16[1,5,1024]{2,1,0:T(8,128)(2,1)S(1)}, bf16[1,5,1024]{2,1,0:T(8,128)(2,1)S(1)}, u32[]{:S(2)}, u32[]{:S(2)}) collective-permute-start(bf16[1,5,1024]{2,1,0:T(8,128)(2,1)S(1)} %get-tuple-element.19), channel_id=1, source_target_pairs={{0,18},{2,16},{4,22},{6,20},{8,26},{10,24},{12,30},{14,28},{16,2},... | collective-permute-start | bytes 30728 | tf_op jit(solution)/shard_map/ppermute | solution.py:202
  111.1 3.1 %collective-permute-start.10 = (bf16[1,5,1024]{2,1,0:T(8,128)(2,1)S(1)}, bf16[1,5,1024]{2,1,0:T(8,128)(2,1)S(1)}, u32[]{:S(2)}, u32[]{:S(2)}) collective-permute-start(bf16[1,5,1024]{2,1,0:T(8,128)(2,1)S(1)} %get-tuple-element.17), channel_id=1, source_target_pairs={{0,22},{2,20},{4,18},{6,16},{8,30},{10,28},{12,26},{14,24},{16,6},... | collective-permute-start | bytes 30728 | tf_op jit(solution)/shard_map/ppermute | solution.py:202
  114.2 3.7 %collective-permute-start.12 = (bf16[1,5,1024]{2,1,0:T(8,128)(2,1)S(1)}, bf16[1,5,1024]{2,1,0:T(8,128)(2,1)S(1)}, u32[]{:S(2)}, u32[]{:S(2)}) collective-permute-start(bf16[1,5,1024]{2,1,0:T(8,128)(2,1)S(1)} %get-tuple-element.15), channel_id=1, source_target_pairs={{0,26},{2,24},{4,30},{6,28},{8,18},{10,16},{12,22},{14,20},{16,10}... | collective-permute-start | bytes 30728 | tf_op jit(solution)/shard_map/ppermute | solution.py:202
  118.4 3.8 %collective-permute-start.14 = (bf16[1,5,1024]{2,1,0:T(8,128)(2,1)S(1)}, bf16[1,5,1024]{2,1,0:T(8,128)(2,1)S(1)}, u32[]{:S(2)}, u32[]{:S(2)}) collective-permute-start(bf16[1,5,1024]{2,1,0:T(8,128)(2,1)S(1)} %get-tuple-element.13), channel_id=1, source_target_pairs={{0,30},{2,28},{4,26},{6,24},{8,22},{10,20},{12,18},{14,16},{16,14}... | collective-permute-start | bytes 30728 | tf_op jit(solution)/shard_map/ppermute | solution.py:202
  122.3 2.2 %collective-permute-done.13 = bf16[1,5,1024]{2,1,0:T(8,128)(2,1)S(1)} collective-permute-done((bf16[1,5,1024]{2,1,0:T(8,128)(2,1)S(1)}, bf16[1,5,1024]{2,1,0:T(8,128)(2,1)S(1)}, u32[]{:S(2)}, u32[]{:S(2)}) %collective-permute-start.13) | collective-permute-done | bytes 10272 | tf_op jit(solution)/shard_map/ppermute | solution.py:202
  125.2 0.6 gather_fusion.1
  125.9 60.0 %all-reduce.4.cloned.1.call-done = f32[64,1024]{1,0:T(8,128)} async-done(((f32[64,1024]{1,0:T(8,128)}), f32[64,1024]{1,0:T(8,128)}) %all-reduce.4.cloned.1.call-update) | async-done | bytes 262160
  186.0 0.9 multiply_reduce_fusion.2
  186.9 1.4 fusion.38
  (120 shorter events, 7.1 us)
Async XLA Ops:
  7.2 35.6 %copy-start = (bf16[4,1024,256]{2,1,0:T(8,128)(2,1)S(1)}, bf16[4,1024,256]{2,1,0:T(8,128)(2,1)}, u32[]{:S(2)}) copy-start(bf16[4,1024,256]{2,1,0:T(8,128)(2,1)} %param.26) | copy-start | bytes 6291460
  7.2 36.2 %copy-start.3 = (bf16[4,32,1024]{2,1,0:T(8,128)(2,1)S(1)}, bf16[4,32,1024]{2,1,0:T(8,128)(2,1)}, u32[]{:S(2)}) copy-start(bf16[4,32,1024]{2,1,0:T(8,128)(2,1)} %param.27) | copy-start | bytes 786436
  16.4 11.9 %all-to-all-start.1 = ((bf16[2,2,256]{2,1,0:T(2,128)(2,1)}), bf16[2,2,256]{2,1,0:T(2,128)(2,1)S(1)}, u32[]{:S(2)}, u32[]{:S(2)}) async-start(bf16[2,2,256]{2,1,0:T(2,128)(2,1)} %reshape.314), calls=%async_computation.1 | async-start | bytes 4096 | tf_op jit(solution)/shard_map/all_to_all | solution.py:152
  28.3 7.1 %all-to-all-start.2 = ((f32[2,4,128]{2,1,0:T(4,128)}), f32[2,4,128]{2,1,0:T(4,128)S(1)}, u32[]{:S(2)}, u32[]{:S(2)}) async-start(f32[2,4,128]{2,1,0:T(4,128)} %bitcast.9), calls=%async_computation.2 | async-start | bytes 8192 | tf_op jit(solution)/shard_map/all_to_all | solution.py:141
  35.4 7.1 %all-to-all-start = ((bf16[8,4,256]{2,1,0:T(4,128)(2,1)}), bf16[8,4,256]{2,1,0:T(4,128)(2,1)S(1)}, u32[]{:S(2)}, u32[]{:S(2)}) async-start(bf16[8,4,256]{2,1,0:T(4,128)(2,1)} %copy.49), calls=%async_computation | async-start | bytes 32768 | tf_op jit(solution)/shard_map/all_to_all | solution.py:151
  43.4 5.0 %copy-start.13 = (u32[32]{0:T(128)S(1)}, u32[32]{0:T(128)}, u32[]{:S(2)}) copy-start(u32[32]{0:T(128)} %constant.91) | copy-start | bytes 388
  43.4 5.6 %copy-start.12 = (u32[32]{0:T(128)S(1)}, u32[32]{0:T(128)}, u32[]{:S(2)}) copy-start(u32[32]{0:T(128)} %constant.95) | copy-start | bytes 388
  43.4 8.8 %copy-start.4 = (bf16[4,256,64]{1,2,0:T(8,128)(2,1)S(1)}, bf16[4,256,64]{1,2,0:T(8,128)(2,1)}, u32[]{:S(2)}) copy-start(bf16[4,256,64]{1,2,0:T(8,128)(2,1)} %param.37) | copy-start | bytes 393220
  43.5 17.8 %copy-start.5 = (bf16[4,1024]{1,0:T(4,128)(2,1)S(1)}, bf16[4,1024]{1,0:T(4,128)(2,1)}, u32[]{:S(2)}) copy-start(bf16[4,1024]{1,0:T(4,128)(2,1)} %param.24) | copy-start | bytes 24580
  43.5 17.8 %copy-start.8 = (f32[1024]{0:T(1024)S(1)}, f32[1024]{0:T(1024)}, u32[]{:S(2)}) copy-start(f32[1024]{0:T(1024)} %param.30) | copy-start | bytes 12292
  43.5 18.0 %copy-start.6 = (f32[1024]{0:T(1024)S(1)}, f32[1024]{0:T(1024)}, u32[]{:S(2)}) copy-start(f32[1024]{0:T(1024)} %param.47) | copy-start | bytes 12292
  43.5 18.0 %copy-start.7 = (f32[1024]{0:T(1024)S(1)}, f32[1024]{0:T(1024)}, u32[]{:S(2)}) copy-start(f32[1024]{0:T(1024)} %param.31) | copy-start | bytes 12292
  44.4 51.7 %copy-start.1 = (bf16[256,1024]{1,0:T(8,128)(2,1)S(1)}, bf16[256,1024]{1,0:T(8,128)(2,1)}, u32[]{:S(2)}) copy-start(bf16[256,1024]{1,0:T(8,128)(2,1)} %param.46) | copy-start | bytes 1572868
  44.5 51.7 %copy-start.2 = (bf16[256,1024]{1,0:T(8,128)(2,1)S(1)}, bf16[256,1024]{1,0:T(8,128)(2,1)}, u32[]{:S(2)}) copy-start(bf16[256,1024]{1,0:T(8,128)(2,1)} %param.45) | copy-start | bytes 1572868
  45.1 7.1 %all-to-all-start.3 = ((bf16[4,8,256]{2,0,1:T(4,128)(2,1)}), bf16[4,8,256]{2,0,1:T(4,128)(2,1)S(1)}, u32[]{:S(2)}, u32[]{:S(2)}) async-start(bf16[4,8,256]{2,0,1:T(4,128)(2,1)} %copy.55), calls=%async_computation.3 | async-start | bytes 32768 | tf_op jit(solution)/shard_map/all_to_all | solution.py:165
  63.3 35.0 %all-to-all-start.4 = ((bf16[16,5,1024]{2,1,0:T(8,128)(2,1)}), bf16[16,5,1024]{2,1,0:T(8,128)(2,1)S(1)}, u32[]{:S(2)}, u32[]{:S(2)}) async-start(bf16[16,5,1024]{2,1,0:T(8,128)(2,1)} %reshape.282), calls=%async_computation.4 | async-start | bytes 524288 | tf_op jit(solution)/shard_map/all_to_all | solution.py:192
  69.7 116.3 %all-reduce.4.cloned.1.call-start = ((), (), s32[]{:S(2)}) async-start(), calls=%async_computation.5 | async-start | bytes 524288
  98.3 3.7 %copy-start.11 = (f32[4]{0:T(128)S(1)}, f32[4]{0:T(128)}, u32[]{:S(2)}) copy-start(f32[4]{0:T(128)} %get-tuple-element.3) | copy-start | bytes 52
  99.7 26.1 %copy-start.10 = (f32[4,6]{1,0:T(4,128)S(1)}, f32[4,6]{1,0:T(4,128)}, u32[]{:S(2)}) copy-start(f32[4,6]{1,0:T(4,128)} %param.40) | copy-start | bytes 292
  99.7 87.3 %copy-start.9 = (f32[1024]{0:T(1024)S(1)}, f32[1024]{0:T(1024)}, u32[]{:S(2)}) copy-start(f32[1024]{0:T(1024)} %param.32) | copy-start | bytes 12292
  101.6 4.0 %collective-permute-start = (bf16[1,5,1024]{2,1,0:T(8,128)(2,1)S(1)}, bf16[1,5,1024]{2,1,0:T(8,128)(2,1)S(1)}, u32[]{:S(2)}, u32[]{:S(2)}) collective-permute-start(bf16[1,5,1024]{2,1,0:T(8,128)(2,1)S(1)} %get-tuple-element.27), channel_id=1, source_target_pairs={{0,2},{2,0},{4,6},{6,4},{8,10},{10,8},{12,14},{14,12},{16,18},{18,... | collective-permute-start | bytes 30728 | tf_op jit(solution)/shard_map/ppermute | solution.py:202
  102.0 3.9 %collective-permute-start.1 = (bf16[1,5,1024]{2,1,0:T(8,128)(2,1)S(1)}, bf16[1,5,1024]{2,1,0:T(8,128)(2,1)S(1)}, u32[]{:S(2)}, u32[]{:S(2)}) collective-permute-start(bf16[1,5,1024]{2,1,0:T(8,128)(2,1)S(1)} %get-tuple-element.26), channel_id=1, source_target_pairs={{0,4},{2,6},{4,0},{6,2},{8,12},{10,14},{12,8},{14,10},{16,20},{18,... | collective-permute-start | bytes 30728 | tf_op jit(solution)/shard_map/ppermute | solution.py:202
  102.5 5.5 %collective-permute-start.2 = (bf16[1,5,1024]{2,1,0:T(8,128)(2,1)S(1)}, bf16[1,5,1024]{2,1,0:T(8,128)(2,1)S(1)}, u32[]{:S(2)}, u32[]{:S(2)}) collective-permute-start(bf16[1,5,1024]{2,1,0:T(8,128)(2,1)S(1)} %get-tuple-element.25), channel_id=1, source_target_pairs={{0,6},{2,4},{4,2},{6,0},{8,14},{10,12},{12,10},{14,8},{16,22},{18,... | collective-permute-start | bytes 30728 | tf_op jit(solution)/shard_map/ppermute | solution.py:202
  103.6 4.4 %collective-permute-start.3 = (bf16[1,5,1024]{2,1,0:T(8,128)(2,1)S(1)}, bf16[1,5,1024]{2,1,0:T(8,128)(2,1)S(1)}, u32[]{:S(2)}, u32[]{:S(2)}) collective-permute-start(bf16[1,5,1024]{2,1,0:T(8,128)(2,1)S(1)} %get-tuple-element.24), channel_id=1, source_target_pairs={{0,8},{2,10},{4,12},{6,14},{8,0},{10,2},{12,4},{14,6},{16,24},{18,... | collective-permute-start | bytes 30728 | tf_op jit(solution)/shard_map/ppermute | solution.py:202
  103.6 7.3 %collective-permute-start.4 = (bf16[1,5,1024]{2,1,0:T(8,128)(2,1)S(1)}, bf16[1,5,1024]{2,1,0:T(8,128)(2,1)S(1)}, u32[]{:S(2)}, u32[]{:S(2)}) collective-permute-start(bf16[1,5,1024]{2,1,0:T(8,128)(2,1)S(1)} %get-tuple-element.23), channel_id=1, source_target_pairs={{0,10},{2,8},{4,14},{6,12},{8,2},{10,0},{12,6},{14,4},{16,26},{18,... | collective-permute-start | bytes 30728 | tf_op jit(solution)/shard_map/ppermute | solution.py:202
  105.6 5.5 %collective-permute-start.5 = (bf16[1,5,1024]{2,1,0:T(8,128)(2,1)S(1)}, bf16[1,5,1024]{2,1,0:T(8,128)(2,1)S(1)}, u32[]{:S(2)}, u32[]{:S(2)}) collective-permute-start(bf16[1,5,1024]{2,1,0:T(8,128)(2,1)S(1)} %get-tuple-element.22), channel_id=1, source_target_pairs={{0,12},{2,14},{4,8},{6,10},{8,4},{10,6},{12,0},{14,2},{16,28},{18,... | collective-permute-start | bytes 30728 | tf_op jit(solution)/shard_map/ppermute | solution.py:202
  105.9 8.3 %collective-permute-start.6 = (bf16[1,5,1024]{2,1,0:T(8,128)(2,1)S(1)}, bf16[1,5,1024]{2,1,0:T(8,128)(2,1)S(1)}, u32[]{:S(2)}, u32[]{:S(2)}) collective-permute-start(bf16[1,5,1024]{2,1,0:T(8,128)(2,1)S(1)} %get-tuple-element.21), channel_id=1, source_target_pairs={{0,14},{2,12},{4,10},{6,8},{8,6},{10,4},{12,2},{14,0},{16,30},{18,... | collective-permute-start | bytes 30728 | tf_op jit(solution)/shard_map/ppermute | solution.py:202
  108.0 6.3 %collective-permute-start.7 = (bf16[1,5,1024]{2,1,0:T(8,128)(2,1)S(1)}, bf16[1,5,1024]{2,1,0:T(8,128)(2,1)S(1)}, u32[]{:S(2)}, u32[]{:S(2)}) collective-permute-start(bf16[1,5,1024]{2,1,0:T(8,128)(2,1)S(1)} %get-tuple-element.20), channel_id=1, source_target_pairs={{0,16},{2,18},{4,20},{6,22},{8,24},{10,26},{12,28},{14,30},{16,0},... | collective-permute-start | bytes 30728 | tf_op jit(solution)/shard_map/ppermute | solution.py:202
  108.0 10.0 %collective-permute-start.8 = (bf16[1,5,1024]{2,1,0:T(8,128)(2,1)S(1)}, bf16[1,5,1024]{2,1,0:T(8,128)(2,1)S(1)}, u32[]{:S(2)}, u32[]{:S(2)}) collective-permute-start(bf16[1,5,1024]{2,1,0:T(8,128)(2,1)S(1)} %get-tuple-element.19), channel_id=1, source_target_pairs={{0,18},{2,16},{4,22},{6,20},{8,26},{10,24},{12,30},{14,28},{16,2},... | collective-permute-start | bytes 30728 | tf_op jit(solution)/shard_map/ppermute | solution.py:202
  110.9 7.5 %collective-permute-start.9 = (bf16[1,5,1024]{2,1,0:T(8,128)(2,1)S(1)}, bf16[1,5,1024]{2,1,0:T(8,128)(2,1)S(1)}, u32[]{:S(2)}, u32[]{:S(2)}) collective-permute-start(bf16[1,5,1024]{2,1,0:T(8,128)(2,1)S(1)} %get-tuple-element.18), channel_id=1, source_target_pairs={{0,20},{2,22},{4,16},{6,18},{8,28},{10,30},{12,24},{14,26},{16,4},... | collective-permute-start | bytes 30728 | tf_op jit(solution)/shard_map/ppermute | solution.py:202
  111.1 11.1 %collective-permute-start.10 = (bf16[1,5,1024]{2,1,0:T(8,128)(2,1)S(1)}, bf16[1,5,1024]{2,1,0:T(8,128)(2,1)S(1)}, u32[]{:S(2)}, u32[]{:S(2)}) collective-permute-start(bf16[1,5,1024]{2,1,0:T(8,128)(2,1)S(1)} %get-tuple-element.17), channel_id=1, source_target_pairs={{0,22},{2,20},{4,18},{6,16},{8,30},{10,28},{12,26},{14,24},{16,6},... | collective-permute-start | bytes 30728 | tf_op jit(solution)/shard_map/ppermute | solution.py:202
  114.2 8.0 %collective-permute-start.11 = (bf16[1,5,1024]{2,1,0:T(8,128)(2,1)S(1)}, bf16[1,5,1024]{2,1,0:T(8,128)(2,1)S(1)}, u32[]{:S(2)}, u32[]{:S(2)}) collective-permute-start(bf16[1,5,1024]{2,1,0:T(8,128)(2,1)S(1)} %get-tuple-element.16), channel_id=1, source_target_pairs={{0,24},{2,26},{4,28},{6,30},{8,16},{10,18},{12,20},{14,22},{16,8},... | collective-permute-start | bytes 30728 | tf_op jit(solution)/shard_map/ppermute | solution.py:202
  114.2 8.0 %collective-permute-start.12 = (bf16[1,5,1024]{2,1,0:T(8,128)(2,1)S(1)}, bf16[1,5,1024]{2,1,0:T(8,128)(2,1)S(1)}, u32[]{:S(2)}, u32[]{:S(2)}) collective-permute-start(bf16[1,5,1024]{2,1,0:T(8,128)(2,1)S(1)} %get-tuple-element.15), channel_id=1, source_target_pairs={{0,26},{2,24},{4,30},{6,28},{8,18},{10,16},{12,22},{14,20},{16,10}... | collective-permute-start | bytes 30728 | tf_op jit(solution)/shard_map/ppermute | solution.py:202
  118.0 6.5 %collective-permute-start.13 = (bf16[1,5,1024]{2,1,0:T(8,128)(2,1)S(1)}, bf16[1,5,1024]{2,1,0:T(8,128)(2,1)S(1)}, u32[]{:S(2)}, u32[]{:S(2)}) collective-permute-start(bf16[1,5,1024]{2,1,0:T(8,128)(2,1)S(1)} %get-tuple-element.14), channel_id=1, source_target_pairs={{0,28},{2,30},{4,24},{6,26},{8,20},{10,22},{12,16},{14,18},{16,12}... | collective-permute-start | bytes 30728 | tf_op jit(solution)/shard_map/ppermute | solution.py:202
  118.4 6.1 %collective-permute-start.14 = (bf16[1,5,1024]{2,1,0:T(8,128)(2,1)S(1)}, bf16[1,5,1024]{2,1,0:T(8,128)(2,1)S(1)}, u32[]{:S(2)}, u32[]{:S(2)}) collective-permute-start(bf16[1,5,1024]{2,1,0:T(8,128)(2,1)S(1)} %get-tuple-element.13), channel_id=1, source_target_pairs={{0,30},{2,28},{4,26},{6,24},{8,22},{10,20},{12,18},{14,16},{16,14}... | collective-permute-start | bytes 30728 | tf_op jit(solution)/shard_map/ppermute | solution.py:202
Sparse Core Ops, SparseCore 0:
  98.4 87.5 all-reduce.3
